TPU v7x, 128 devices: a whole 4x4x4 slice. The times are simulated.
128 devices in a mesh: kv: 16 (over z, y), tp: 8 (over x, core).
Axes of the slice: x: 4, y: 4, z: 4, core: 2. Of those that a mesh axis runs over, the one named last changes fastest.
Arguments:
- tokens: bfloat16 [256, 4096], P(None, ('kv', 'tp')), may hold values from -64 to 64
- mix_gain: float32 [4096], P('kv'), may hold values from 0.1 to 1.9
- w_query: bfloat16 [4096, 3072], P('kv', 'tp'), may hold values from -0.09375 to 0.09375
- w_key: bfloat16 [4096, 3072], P('kv', 'tp'), may hold values from -0.09375 to 0.09375
- w_value: bfloat16 [4096, 3072], P('kv', 'tp'), may hold values from -0.09375 to 0.09375
- w_gate: bfloat16 [4096, 3072], P('kv', 'tp'), may hold values from -0.09375 to 0.09375
- w_beta: bfloat16 [4096, 24], P('kv'), may hold values from -0.09375 to 0.09375
- w_decay: bfloat16 [4096, 24], P('kv'), may hold values from -0.09375 to 0.09375
- decay_rate: float32 [24], P('tp'), may hold values from 0.15 to 1.5
- out_gain: float32 [128], replicated, may hold values from 0.1 to 1.9
- state: float32 [256, 24, 128, 128], P('kv', 'tp'), may hold values from -0.6 to 0.6
- w_out: bfloat16 [3072, 4096], P('tp', 'kv'), may hold values from -0.109375 to 0.109375
- mlp_gain: float32 [4096], replicated, may hold values from 0.1 to 1.9
- w_up: bfloat16 [4096, 16384], P(None, ('kv', 'tp')), may hold values from -0.09375 to 0.09375
- w_down: bfloat16 [16384, 4096], P(('kv', 'tp')), may hold values from -0.1875 to 0.1875
Outputs:
- mixed: bfloat16 [256, 4096], P(None, ('kv', 'tp'))
- new_state: float32 [256, 24, 128, 128], P('kv', 'tp')
All inputs are finite; a program needn't handle non-finite values.
Results may differ from a plain program's by a relative error of at most 0.0063.
Values may be sent and summed in bfloat16 or wider, within the bound.
A program may use at most 64 MiB of HBM per device.

v0:
```python
import math
import jax
import jax.numpy as jnp
from jax import lax
from jax.sharding import Mesh
from jax.sharding import PartitionSpec as P

D = 4096
TP = ("tp_0", "tp_1")
KV = ("kv_0", "kv_1")
KV_TP = ("kv_0", "kv_1", "tp_0", "tp_1")
EPSILON = 1e-06


def side_by_side(arrays, axis, dim, along):
    widths = [math.prod(a.shape[along:]) for a in arrays]
    both = jnp.concatenate(
        [a.reshape(*a.shape[:along], w) for a, w in zip(arrays, widths)], axis=along
    )
    filled = lax.psum_scatter(both, axis, scatter_dimension=dim, tiled=True)
    pieces = jnp.split(filled, [sum(widths[:k]) for k in range(1, len(widths))], axis=along)
    return tuple(
        (b.reshape(*filled.shape[:along], *a.shape[along:]) for a, b in zip(arrays, pieces))
    )


def in_blocks(value, dim, count):
    shape = value.shape
    pieces = value.reshape(*shape[:dim], count, shape[dim] // count, *shape[dim + 1 :])
    return jnp.moveaxis(pieces, dim, 0)


def summed_on_arrival(value, axis, dim):
    count = lax.axis_size(axis)
    pieces = lax.all_to_all(in_blocks(value, dim, count), axis, 0, 0, tiled=True)
    return jnp.sum(pieces, axis=0)


def joined_along(pieces, dim):
    shape = list(pieces.shape[1:])
    shape[dim] *= pieces.shape[0]
    return jnp.moveaxis(pieces, 0, dim).reshape(shape)


def exchange_in_order(pieces, axes, sequence):
    inside = pieces.shape[1:]
    filled = pieces.reshape(*(lax.axis_size(a) for a in axes), *inside)
    for k in sequence:
        filled = lax.all_to_all(filled, axes[k], k, k, tiled=True)
    return filled.reshape(-1, *inside)


def exchange_by_chip(value, groups, sequence, split_dim, concat_dim):
    count = lax.axis_size(groups[0]) * lax.axis_size(groups[1])
    pieces = in_blocks(value, split_dim, count)
    return joined_along(exchange_in_order(pieces, groups, sequence), concat_dim)


def head_norm(values):
    return values * lax.rsqrt(jnp.sum(values * values, axis=-1, keepdims=True) + EPSILON)


def feed_forward(segment, mlp_gain, w_up, w_down):
    segment_f = segment.astype(jnp.float32)
    normed_mlp = (
        segment_f
        * lax.rsqrt(jnp.mean(segment_f * segment_f, axis=1, keepdims=True) + EPSILON)
        * mlp_gain[None, :]
    ).astype(jnp.bfloat16)
    hidden = jnp.square(
        jax.nn.relu(jnp.dot(normed_mlp, w_up, preferred_element_type=jnp.float32))
    ).astype(jnp.bfloat16)
    return jnp.dot(hidden, w_down, preferred_element_type=jnp.float32)


def local(
    tokens,
    mix_gain,
    w_query,
    w_key,
    w_value,
    w_gate,
    w_beta,
    w_decay,
    decay_rate,
    out_gain,
    state,
    w_out,
    mlp_gain,
    w_up,
    w_down,
):
    local_rows = state.shape[0]
    local_heads = decay_rate.shape[0]
    head_size = state.shape[2]
    all_heads = w_beta.shape[1]
    columns = lax.all_gather(tokens, TP, axis=1, tiled=True)
    columns_f = columns.astype(jnp.float32)
    normed = (columns_f * mix_gain[None, :]).astype(jnp.bfloat16)
    part_query = jnp.dot(normed, w_query, preferred_element_type=jnp.float32)
    part_key = jnp.dot(normed, w_key, preferred_element_type=jnp.float32)
    part_value = jnp.dot(normed, w_value, preferred_element_type=jnp.float32)
    part_gate = jnp.dot(normed, w_gate, preferred_element_type=jnp.float32)
    part_rates = jnp.dot(
        normed, jnp.concatenate([w_beta, w_decay], axis=1), preferred_element_type=jnp.float32
    )
    summed = side_by_side(
        (
            part_query,
            part_key,
            part_value,
            part_gate,
            part_rates,
            jnp.sum(columns_f * columns_f, axis=1),
        ),
        KV,
        0,
        1,
    )
    own_squares = summed[5]
    row_scale = lax.rsqrt(own_squares / D + EPSILON)[:, None]
    shape_heads = (local_rows, local_heads, head_size)
    query = head_norm(jax.nn.silu((summed[0] * row_scale).reshape(shape_heads))) * head_size ** (
        -0.5
    )
    key = head_norm(jax.nn.silu((summed[1] * row_scale).reshape(shape_heads)))
    value = jax.nn.silu((summed[2] * row_scale).reshape(shape_heads))
    gate_raw = (summed[3] * row_scale).reshape(shape_heads)
    rates = summed[4] * row_scale
    head_start = lax.axis_index(TP) * local_heads
    beta = jax.nn.sigmoid(lax.dynamic_slice_in_dim(rates, head_start, local_heads, 1))
    decay_raw = lax.dynamic_slice_in_dim(rates, all_heads + head_start, local_heads, 1)
    decay = jnp.exp(-decay_rate[None, :] * jax.nn.softplus(decay_raw))
    faded = state * decay[:, :, None, None]
    recalled = jnp.einsum("bhkv,bhk->bhv", faded, key, precision=lax.Precision.HIGHEST)
    change = beta[:, :, None] * (value - recalled)
    new_state = faded + key[:, :, :, None] * change[:, :, None, :]
    readout = jnp.einsum("bhkv,bhk->bhv", new_state, query, precision=lax.Precision.HIGHEST)
    scaled = (
        readout
        * lax.rsqrt(jnp.mean(readout * readout, axis=-1, keepdims=True) + EPSILON)
        * out_gain
    )
    merged = (
        (scaled * jax.nn.silu(gate_raw))
        .reshape(local_rows, local_heads * head_size)
        .astype(jnp.bfloat16)
    )
    partial_out = jnp.dot(
        lax.all_gather(merged, KV, axis=0, tiled=True), w_out, preferred_element_type=jnp.float32
    )
    branch_sum = summed_on_arrival(partial_out, TP, 1)
    residual = (tokens.astype(jnp.float32) + branch_sum).astype(jnp.bfloat16)
    whole_rows = lax.all_gather(residual, KV_TP, axis=1, tiled=True)
    partial_mlp = feed_forward(whole_rows, mlp_gain, w_up, w_down)
    row_branch = lax.psum_scatter(partial_mlp, KV_TP, scatter_dimension=0, tiled=True)
    own_count = row_branch.shape[0]
    own_rows = lax.dynamic_slice_in_dim(whole_rows, lax.axis_index(KV_TP) * own_count, own_count, 0)
    finished = (own_rows.astype(jnp.float32) + row_branch).astype(jnp.bfloat16)
    mixed = exchange_by_chip(finished, (("kv_0", "kv_1", "tp_0"), "tp_1"), (1, 0), 1, 0)
    return (mixed, new_state)


def solution(mesh):
    torus = Mesh(mesh.devices.reshape(4, 4, 4, 2), ("kv_0", "kv_1", "tp_0", "tp_1"))
    in_specs = (
        P(None, KV_TP),
        P(KV),
        P(KV, TP),
        P(KV, TP),
        P(KV, TP),
        P(KV, TP),
        P(KV, None),
        P(KV, None),
        P(TP),
        P(),
        P(KV, TP, None, None),
        P(TP, KV),
        P(),
        P(None, KV_TP),
        P(KV_TP, None),
    )
    out_specs = (P(None, KV_TP), P(KV, TP, None, None))
    return jax.shard_map(local, mesh=torus, in_specs=in_specs, out_specs=out_specs, check_vma=False)
```

profile of v0, /device:TPU:0, one launch (start us, length us, event | category | flops | bytes accessed | tf_op | source)
XLA Modules:
  0.0 419.6 jit_solution(876211718287899662)
XLA Ops:
  7.3 13.6 %all_gather.9 = bf16[256,256]{0,1:T(8,128)(2,1)S(1)} all-gather(bf16[256,32]{0,1:T(8,128)(2,1)} %param.15), channel_id=1, replica_groups=mesh['kv_0'=4,'kv_1'=4,'tp_0'=4,'tp_1'=2] {'tp_0','tp_1'}, dimensions={1}, use_global_device_ids=true | all-gather | bytes 147456 | tf_op jit(solution)/shard_map/all_gather | solution.py:97
  20.8 0.1 fusion.23
  20.9 0.1 copy.42
  21.0 1.3 fusion.51
  22.3 1.3 fusion.49
  23.6 1.3 fusion.47
  24.9 1.3 fusion.53
  26.2 0.3 fusion.32
  26.5 1.4 concatenate.7
  27.9 0.0 all-gather.2.cloned.1.call-start
  28.0 0.6 dynamic-slice
  29.3 89.5 %all-reduce.5.cloned.1.call-done = f32[256,1585]{1,0:T(8,128)} async-done(((f32[256,1585]{1,0:T(8,128)}), f32[256,1585]{1,0:T(8,128)}) %all-reduce.5.cloned.1.call-update) | async-done | bytes 1623056
  118.8 0.9 fusion.43
  119.7 0.9 dynamic-slice_multiply_fusion.1
  120.6 0.1 multiply_reduce_fusion.1
  120.8 0.1 fusion.65
  120.8 0.1 broadcast_multiply_fusion
  121.0 0.1 multiply_reduce_fusion
  121.1 0.1 multiply_bitcast_fusion
  121.2 0.9 dynamic-slice_multiply_fusion.5
  122.1 0.1 add_divide_fusion
  122.3 4.8 %fusion.3 = f32[16,3,1,128]{3,2,1,0:T(1,128)S(1)} fusion(f32[16,3,128,128]{3,2,1,0:T(8,128)} %param.25, f32[16,3]{1,0:T(8,128)S(1)} %get-tuple-element.15, f32[16,3,128,1]{2,1,0,3:T(4,128)S(1)} %fusion.65), kind=kOutput, calls=%fused_computation.6 | convolution fusion | flops 10223616 | bytes 3195072 | tf_op jit(solution)/shard_map/bhkv,bhk->bhv/dot_general | solution.py:135
  127.0 0.1 fusion.30
  127.1 1.1 multiply_add_fusion
  128.3 1.7 copy-done.3
  129.9 2.8 fusion.36
  132.7 0.1 fusion.28
  132.8 0.1 fusion.31
  132.9 23.2 %all_gather.10 = bf16[256,384]{1,0:T(8,128)(2,1)S(1)} all-gather(bf16[16,384]{1,0:T(8,128)(2,1)S(1)} %bitcast.49), channel_id=1, replica_groups=mesh['kv_0'=4,'kv_1'=4,'tp_0'=4,'tp_1'=2] {'kv_0','kv_1'}, dimensions={0}, use_global_device_ids=true | all-gather | bytes 208896 | tf_op jit(solution)/shard_map/all_gather | solution.py:150
  156.1 0.3 fusion.55
  156.4 11.6 %all_to_all.15 = f32[8,256,32]{1,2,0:T(8,128)S(1)} all-to-all(f32[8,256,32]{1,2,0:T(8,128)S(1)} %bitcast.43), channel_id=1, replica_groups=mesh['kv_0'=4,'kv_1'=4,'tp_0'=4,'tp_1'=2] {'tp_0','tp_1'}, dimensions={0} | all-to-all | bytes 524288 | tf_op jit(solution)/shard_map/all_to_all | solution.py:35
  168.0 0.6 add_convert_fusion
  168.7 0.2 all-reduce.7.cloned.1.call-start
  168.9 61.9 %all-gather.2.cloned.1.call-done = bf16[256,4096]{0,1:T(8,128)(2,1)} async-done(((bf16[256,32]{0,1:T(8,128)(2,1)}), bf16[256,4096]{0,1:T(8,128)(2,1)}) %all-gather.2.cloned.1.call-update) | async-done | bytes 2097168 | tf_op jit(solution)/shard_map/all_gather | solution.py:154
  230.8 2.3 fusion
  233.2 5.3 %fusion.20 = f32[256,4096]{1,0:T(8,128)} fusion(bf16[128,4096]{1,0:T(8,128)(2,1)S(1)} %copy-done, bf16[4096,128]{1,0:T(8,128)(2,1)} %param.28, bf16[256,4096]{0,1:T(8,128)(2,1)S(1)} %copy-done.1, f32[4096]{0:T(1024)S(1)} %copy-done.7, f32[256]{0:T(256)S(1)} %add_rsqrt_fusion.3), kind=kOutput, calls=%fused_computation.15 | convolution fusion | flops 541163520 | bytes 8406016 | tf_op jit(solution)/shard_map/dot_general | solution.py:73
  238.5 1.4 constant_dynamic-slice_fusion
  240.0 1.6 copy.52
  241.6 148.9 %all-reduce.7.cloned.1.call-done = f32[256,4096]{1,0:T(8,128)} async-done(((f32[256,4096]{1,0:T(8,128)}), f32[256,4096]{1,0:T(8,128)}) %all-reduce.7.cloned.1.call-update) | async-done | bytes 4194320
  390.5 0.9 fusion.27
  391.4 0.1 reshape.86
  391.5 0.1 copy.44
  391.6 0.1 reshape.94
  391.7 3.7 all_to_all.16
  395.4 0.1 reshape.95
  395.5 0.1 copy.45
  395.6 16.7 %all_to_all.17 = bf16[64,2,2,32]{3,2,1,0:T(2,128)(2,1)S(1)} all-to-all(bf16[64,2,2,32]{3,2,1,0:T(2,128)(2,1)S(1)} %copy.45), channel_id=1, replica_groups=mesh['kv_0'=4,'kv_1'=4,'tp_0'=4,'tp_1'=2] {'kv_0','kv_1','tp_0'}, dimensions={0} | all-to-all | bytes 32768 | tf_op jit(solution)/shard_map/all_to_all | solution.py:49
  412.3 0.7 copy.46
  (40 shorter events, 0.3 us)
Async XLA Ops:
  7.2 226.0 %copy-start = (bf16[128,4096]{1,0:T(8,128)(2,1)S(1)}, bf16[128,4096]{1,0:T(8,128)(2,1)}, u32[]{:S(2)}) copy-start(bf16[128,4096]{1,0:T(8,128)(2,1)} %param.29) | copy-start | bytes 3145732
  7.2 19.0 %copy-start.6 = (f32[256]{0:T(256)S(1)}, f32[256]{0:T(256)}, u32[]{:S(2)}) copy-start(f32[256]{0:T(256)} %param.16) | copy-start | bytes 3076
  7.2 19.0 %copy-start.8 = (bf16[256,24]{0,1:T(8,128)(2,1)S(1)}, bf16[256,24]{0,1:T(8,128)(2,1)}, u32[]{:S(2)}) copy-start(bf16[256,24]{0,1:T(8,128)(2,1)} %param.22) | copy-start | bytes 36868
  7.2 19.0 %copy-start.9 = (bf16[256,24]{0,1:T(8,128)(2,1)S(1)}, bf16[256,24]{0,1:T(8,128)(2,1)}, u32[]{:S(2)}) copy-start(bf16[256,24]{0,1:T(8,128)(2,1)} %param.21) | copy-start | bytes 36868
  7.2 111.6 %all-reduce.5.cloned.1.call-start = ((), (), s32[]{:S(2)}) async-start(), calls=%async_computation.4 | async-start | bytes 3407872
  24.9 3.2 copy-start.11
  24.9 3.2 copy-start.12
  27.9 202.9 %all-gather.2.cloned.1.call-start = ((), (), s32[]{:S(2)}) async-start(), calls=%async_computation.3 | async-start | bytes 2113536 | tf_op jit(solution)/shard_map/all_gather | solution.py:154
  121.2 5.9 %copy-start.2 = (f32[16,3,128,128]{3,2,1,0:T(8,128)S(1)}, f32[16,3,128,128]{3,2,1,0:T(8,128)}, u32[]{:S(2)}) copy-start(f32[16,3,128,128]{3,2,1,0:T(8,128)} %param.25) | copy-start | bytes 9437188
  128.3 1.7 copy-start.3
  129.9 2.9 copy-start.10
  129.9 26.2 %copy-start.4 = (bf16[384,256]{1,0:T(8,128)(2,1)S(1)}, bf16[384,256]{1,0:T(8,128)(2,1)}, u32[]{:S(2)}) copy-start(bf16[384,256]{1,0:T(8,128)(2,1)} %param.26) | copy-start | bytes 589828
  129.9 38.1 %copy-start.5 = (bf16[256,32]{0,1:T(8,128)(2,1)S(1)}, bf16[256,32]{0,1:T(8,128)(2,1)}, u32[]{:S(2)}) copy-start(bf16[256,32]{0,1:T(8,128)(2,1)} %param.15) | copy-start | bytes 49156
  129.9 103.2 %copy-start.7 = (f32[4096]{0:T(1024)S(1)}, f32[4096]{0:T(1024)}, u32[]{:S(2)}) copy-start(f32[4096]{0:T(1024)} %param.27) | copy-start | bytes 49156
  168.7 221.8 %all-reduce.7.cloned.1.call-start = ((), (), s32[]{:S(2)}) async-start(), calls=%async_computation.5 | async-start | bytes 8388608
  230.8 2.3 copy-start.1
Sparse Core Ops, SparseCore 0:
  28.1 90.6 all-reduce.4
  168.8 62.0 all-gather.1
  238.7 151.7 all-reduce.6
where the time goes:
time: 420 us
  waiting for transfers between devices  300 us (71%)
  blocking collectives  68.7 us (16%)
  matrix products  18.6 us (4%)
  between operations  14.8 us (4%)
  other arithmetic  8.67 us (2%)
  local copies, waits for them, and re-layouts  8.14 us (2%)
    unnamed x5, waiting for transfers between devices  238 us
    all_gather x1, waiting for transfers between devices, local(): whole_rows = lax.all_gather(residual, KV_TP, axis=1, tiled=True)  61.9 us
    all_gather x1, blocking collectives, local(): lax.all_gather(merged, KV, axis=0, tiled=True)  23.2 us
    all_to_all x2, blocking collectives, exchange_in_order(): filled = lax.all_to_all(filled, axes[k], k, k, tiled=True)  20.4 us
    all_gather x1, blocking collectives, local(): columns = lax.all_gather(tokens, TP, axis=1, tiled=True)  13.6 us
    all_to_all x1, blocking collectives, summed_on_arrival(): lax.all_to_all(in_blocks(value, dim, count), axis, 0, 0, tiled=True)  11.6 us
  transfers between devices with their start and end apart: 3, of which 3 were waited for; matrix products, arithmetic and copies ran while one was open for 1% of the time, Pallas kernels for 0%

commit v1 on v0

--- a/solution.py
+++ b/solution.py
@@ -147,7 +147,9 @@
         .astype(jnp.bfloat16)
     )
     partial_out = jnp.dot(
-        lax.all_gather(merged, KV, axis=0, tiled=True), w_out, preferred_element_type=jnp.float32
+        jnp.concatenate(lax.all_to_all(jnp.stack([merged] * lax.axis_size(KV)), KV, 0, 0), axis=0),
+        w_out,
+        preferred_element_type=jnp.float32,
     )
     branch_sum = summed_on_arrival(partial_out, TP, 1)
     residual = (tokens.astype(jnp.float32) + branch_sum).astype(jnp.bfloat16)

time: 420 us -> 410 us (0.976)
  blocking collectives: 68.7 us -> 45.5 us
  waiting for transfers between devices: 300 us -> 308 us
  starting transfers between devices: 0.3 us -> 5.42 us
    all_gather x1 -> x0, blocking collectives: 23.2 us -> none  [local(): lax.all_gather(merged, KV, axis=0, tiled=True)]
    all_to_all x0 -> x1, waiting for transfers between devices: none -> 8.11 us  [local(): lax.all_to_all(jnp.stack([merged] * lax.axis_size(KV)), KV, 0, 0)]
    all_to_all x0 -> x1, starting transfers between devices: none -> 5.11 us  [local(): lax.all_to_all(jnp.stack([merged] * lax.axis_size(KV)), KV, 0, 0)]
  transfers between devices with their start and end apart: 3 -> 4, of which waited for: 3 -> 4; matrix products, arithmetic and copies ran while one was open for 1% -> 1% of each run, Pallas kernels for 0% -> 0%
where the time goes in v1:
time: 410 us
  waiting for transfers between devices  308 us (75%)
  blocking collectives  45.5 us (11%)
  matrix products  18.5 us (5%)
  between operations  14.8 us (4%)
  local copies, waits for them, and re-layouts  8.99 us (2%)
  other arithmetic  8.67 us (2%)
  starting transfers between devices  5.42 us (1%)
    unnamed x5, waiting for transfers between devices  239 us
    all_gather x1, waiting for transfers between devices, local(): whole_rows = lax.all_gather(residual, KV_TP, axis=1, tiled=True)  61.1 us
    all_to_all x2, blocking collectives, exchange_in_order(): filled = lax.all_to_all(filled, axes[k], k, k, tiled=True)  20.4 us
    all_gather x1, blocking collectives, local(): columns = lax.all_gather(tokens, TP, axis=1, tiled=True)  13.6 us
    all_to_all x1, blocking collectives, summed_on_arrival(): lax.all_to_all(in_blocks(value, dim, count), axis, 0, 0, tiled=True)  11.6 us
  transfers between devices with their start and end apart: 4, of which 4 were waited for; matrix products, arithmetic and copies ran while one was open for 1% of the time, Pallas kernels for 0%

profile of v1, /device:TPU:0, one launch (start us, length us, event | category | flops | bytes accessed | tf_op | source)
XLA Modules:
  0.0 409.7 jit_solution(11896370815508657656)
XLA Ops:
  7.3 13.6 %all_gather.6 = bf16[256,256]{0,1:T(8,128)(2,1)S(1)} all-gather(bf16[256,32]{0,1:T(8,128)(2,1)} %param.15), channel_id=1, replica_groups=mesh['kv_0'=4,'kv_1'=4,'tp_0'=4,'tp_1'=2] {'tp_0','tp_1'}, dimensions={1}, use_global_device_ids=true | all-gather | bytes 147456 | tf_op jit(solution)/shard_map/all_gather | solution.py:97
  20.9 0.1 copy.46
  21.0 1.3 fusion.51
  22.3 1.3 fusion.49
  23.6 1.3 fusion.47
  24.9 1.3 fusion.53
  26.2 0.3 fusion.32
  26.5 1.4 concatenate.7
  28.0 0.6 dynamic-slice
  29.2 89.5 %all-reduce.5.cloned.1.call-done = f32[256,1585]{1,0:T(8,128)} async-done(((f32[256,1585]{1,0:T(8,128)}), f32[256,1585]{1,0:T(8,128)}) %all-reduce.5.cloned.1.call-update) | async-done | bytes 1623056
  118.8 0.9 fusion.43
  119.7 0.9 dynamic-slice_multiply_fusion.1
  120.6 0.1 multiply_reduce_fusion.1
  120.8 0.1 fusion.64
  120.8 0.1 broadcast_multiply_fusion
  121.0 0.1 multiply_reduce_fusion
  121.1 0.1 multiply_bitcast_fusion
  121.2 0.9 dynamic-slice_multiply_fusion.5
  122.1 0.1 add_divide_fusion
  122.3 4.8 %fusion.3 = f32[16,3,1,128]{3,2,1,0:T(1,128)S(1)} fusion(f32[16,3,128,128]{3,2,1,0:T(8,128)} %param.25, f32[16,3]{1,0:T(8,128)S(1)} %get-tuple-element.15, f32[16,3,128,1]{2,1,0,3:T(4,128)S(1)} %fusion.64), kind=kOutput, calls=%fused_computation.6 | convolution fusion | flops 10223616 | bytes 3195072 | tf_op jit(solution)/shard_map/bhkv,bhk->bhv/dot_general | solution.py:135
  127.1 1.1 multiply_add_fusion
  128.3 1.7 copy-done.3
  129.9 2.8 fusion.36
  132.7 0.1 fusion.28
  132.8 0.1 fusion.31
  132.9 0.7 stack.2
  133.6 5.1 %all-to-all-start = ((bf16[16,16,384]{2,1,0:T(8,128)(2,1)}), bf16[16,16,384]{2,1,0:T(8,128)(2,1)S(1)}, u32[]{:S(2)}, u32[]{:S(2)}) async-start(bf16[16,16,384]{2,1,0:T(8,128)(2,1)} %stack.2), calls=%async_computation | async-start | bytes 393216 | tf_op jit(solution)/shard_map/all_to_all | solution.py:150
  138.8 0.2 copy.47
  139.0 8.1 %all-to-all-done = bf16[16,16,384]{2,1,0:T(8,128)(2,1)S(1)} async-done(((bf16[16,16,384]{2,1,0:T(8,128)(2,1)}), bf16[16,16,384]{2,1,0:T(8,128)(2,1)S(1)}, u32[]{:S(2)}, u32[]{:S(2)}) %all-to-all-start) | async-done | bytes 196640 | tf_op jit(solution)/shard_map/all_to_all | solution.py:150
  147.1 0.2 convolution_bitcast_fusion
  147.3 11.6 %all_to_all.20 = f32[8,256,32]{1,2,0:T(8,128)S(1)} all-to-all(f32[8,256,32]{1,2,0:T(8,128)S(1)} %convolution_bitcast_fusion), channel_id=1, replica_groups=mesh['kv_0'=4,'kv_1'=4,'tp_0'=4,'tp_1'=2] {'tp_0','tp_1'}, dimensions={0} | all-to-all | bytes 524288 | tf_op jit(solution)/shard_map/all_to_all | solution.py:35
  158.9 0.6 add_convert_fusion
  159.6 0.2 all-reduce.7.cloned.1.call-start
  159.8 61.1 %all-gather.2.cloned.1.call-done = bf16[256,4096]{0,1:T(8,128)(2,1)} async-done(((bf16[256,32]{0,1:T(8,128)(2,1)}), bf16[256,4096]{0,1:T(8,128)(2,1)}) %all-gather.2.cloned.1.call-update) | async-done | bytes 2097168 | tf_op jit(solution)/shard_map/all_gather | solution.py:156
  220.9 2.3 fusion
  223.2 5.3 %fusion.20 = f32[256,4096]{1,0:T(8,128)} fusion(bf16[128,4096]{1,0:T(8,128)(2,1)S(1)} %copy-done, bf16[4096,128]{1,0:T(8,128)(2,1)} %param.28, bf16[256,4096]{0,1:T(8,128)(2,1)S(1)} %copy-done.1, f32[4096]{0:T(1024)S(1)} %copy-done.7, f32[256]{0:T(256)S(1)} %add_rsqrt_fusion.3), kind=kOutput, calls=%fused_computation.16 | convolution fusion | flops 541163520 | bytes 8406016 | tf_op jit(solution)/shard_map/dot_general | solution.py:73
  228.6 1.4 constant_dynamic-slice_fusion
  230.0 1.6 copy.57
  231.6 149.0 %all-reduce.7.cloned.1.call-done = f32[256,4096]{1,0:T(8,128)} async-done(((f32[256,4096]{1,0:T(8,128)}), f32[256,4096]{1,0:T(8,128)}) %all-reduce.7.cloned.1.call-update) | async-done | bytes 4194320
  380.6 0.9 fusion.27
  381.5 0.1 reshape.91
  381.6 0.1 copy.49
  381.7 0.1 reshape.100
  381.8 3.7 all_to_all.21
  385.6 0.1 reshape.101
  385.7 0.1 copy.50
  385.8 16.7 %all_to_all.22 = bf16[64,2,2,32]{3,2,1,0:T(2,128)(2,1)S(1)} all-to-all(bf16[64,2,2,32]{3,2,1,0:T(2,128)(2,1)S(1)} %copy.50), channel_id=1, replica_groups=mesh['kv_0'=4,'kv_1'=4,'tp_0'=4,'tp_1'=2] {'kv_0','kv_1','tp_0'}, dimensions={0} | all-to-all | bytes 32768 | tf_op jit(solution)/shard_map/all_to_all | solution.py:49
  402.5 0.7 copy.51
  (43 shorter events, 0.4 us)
Async XLA Ops:
  7.2 216.0 %copy-start = (bf16[128,4096]{1,0:T(8,128)(2,1)S(1)}, bf16[128,4096]{1,0:T(8,128)(2,1)}, u32[]{:S(2)}) copy-start(bf16[128,4096]{1,0:T(8,128)(2,1)} %param.29) | copy-start | bytes 3145732
  7.2 19.0 %copy-start.6 = (f32[256]{0:T(256)S(1)}, f32[256]{0:T(256)}, u32[]{:S(2)}) copy-start(f32[256]{0:T(256)} %param.16) | copy-start | bytes 3076
  7.2 19.0 %copy-start.8 = (bf16[256,24]{0,1:T(8,128)(2,1)S(1)}, bf16[256,24]{0,1:T(8,128)(2,1)}, u32[]{:S(2)}) copy-start(bf16[256,24]{0,1:T(8,128)(2,1)} %param.22) | copy-start | bytes 36868
  7.2 19.0 %copy-start.9 = (bf16[256,24]{0,1:T(8,128)(2,1)S(1)}, bf16[256,24]{0,1:T(8,128)(2,1)}, u32[]{:S(2)}) copy-start(bf16[256,24]{0,1:T(8,128)(2,1)} %param.21) | copy-start | bytes 36868
  7.2 111.6 %all-reduce.5.cloned.1.call-start = ((), (), s32[]{:S(2)}) async-start(), calls=%async_computation.5 | async-start | bytes 3407872
  24.9 3.1 copy-start.11
  24.9 3.1 copy-start.12
  121.2 5.9 %copy-start.2 = (f32[16,3,128,128]{3,2,1,0:T(8,128)S(1)}, f32[16,3,128,128]{3,2,1,0:T(8,128)}, u32[]{:S(2)}) copy-start(f32[16,3,128,128]{3,2,1,0:T(8,128)} %param.25) | copy-start | bytes 9437188
  128.3 1.7 copy-start.3
  129.9 2.9 copy-start.10
  129.9 8.9 %copy-start.4 = (bf16[384,256]{1,0:T(8,128)(2,1)S(1)}, bf16[384,256]{1,0:T(8,128)(2,1)}, u32[]{:S(2)}) copy-start(bf16[384,256]{1,0:T(8,128)(2,1)} %param.26) | copy-start | bytes 589828
  129.9 29.0 %copy-start.5 = (bf16[256,32]{0,1:T(8,128)(2,1)S(1)}, bf16[256,32]{0,1:T(8,128)(2,1)}, u32[]{:S(2)}) copy-start(bf16[256,32]{0,1:T(8,128)(2,1)} %param.15) | copy-start | bytes 49156
  132.7 90.5 %copy-start.7 = (f32[4096]{0:T(1024)S(1)}, f32[4096]{0:T(1024)}, u32[]{:S(2)}) copy-start(f32[4096]{0:T(1024)} %param.27) | copy-start | bytes 49156
  133.6 13.5 %all-to-all-start = ((bf16[16,16,384]{2,1,0:T(8,128)(2,1)}), bf16[16,16,384]{2,1,0:T(8,128)(2,1)S(1)}, u32[]{:S(2)}, u32[]{:S(2)}) async-start(bf16[16,16,384]{2,1,0:T(8,128)(2,1)} %stack.2), calls=%async_computation | async-start | bytes 393216 | tf_op jit(solution)/shard_map/all_to_all | solution.py:150
  138.7 82.1 %all-gather.2.cloned.1.call-start = ((), (), s32[]{:S(2)}) async-start(), calls=%async_computation.4 | async-start | bytes 2113536 | tf_op jit(solution)/shard_map/all_gather | solution.py:156
  159.6 221.0 %all-reduce.7.cloned.1.call-start = ((), (), s32[]{:S(2)}) async-start(), calls=%async_computation.6 | async-start | bytes 8388608
  220.9 2.3 copy-start.1
Sparse Core Ops, SparseCore 0:
  28.1 90.6 all-reduce.4
  159.7 61.1 all-gather.1
  228.7 151.8 all-reduce.6
